TPU v7x, 32 devices: a whole 2x2x4 slice. The times are simulated.
32 devices in a mesh: gr: 2 (over x), fs: 8 (over z, y), tp: 2 (over core).
Axes of the slice: x: 2, y: 2, z: 4, core: 2. Of those that a mesh axis runs over, the one named last changes fastest.
Arguments:
- tokens: bfloat16 [2048, 2048], P(('gr', 'tp')), may hold values from -6 to 6
- norm_gain: float32 [2048], P('fs'), may hold values from 0.1 to 1.9
- up_weight: float32 [2048, 8192], P('fs', ('gr', 'tp')), may hold values from -0.125 to 0.125
- down_weight: float32 [8192, 2048], P('fs', ('gr', 'tp')), may hold values from -0.09375 to 0.09375
Outputs:
- sampler_up: bfloat16 [2048, 8192], P(None, 'fs')
- sampler_down: bfloat16 [8192, 2048], P('fs')
- mixed: bfloat16 [2048, 2048], P(('gr', 'tp'), 'fs')
All inputs are finite; a program needn't handle non-finite values.
Results may differ from a plain program's by a relative error of at most 0.023.
Values may be sent and summed in bfloat16 or wider, within the bound.
A program may use at most 64 MiB of HBM per device.

v0:
```python
import jax
import jax.numpy as jnp
from jax import lax
from jax.sharding import PartitionSpec as P


def per_device(tokens, norm_gain, up_weight, down_weight):
    up_scaled = (norm_gain[:, None] * up_weight).astype(jnp.bfloat16)
    down_half = down_weight.astype(jnp.bfloat16)
    up_columns, down_columns = (
        lax.all_gather(up_scaled, ("gr", "tp"), axis=1, tiled=True),
        lax.all_gather(down_half, ("gr", "tp"), axis=1, tiled=True),
    )
    up_block = lax.all_to_all(up_columns, "fs", split_axis=1, concat_axis=0, tiled=True)
    widened = tokens.astype(jnp.float32)
    normed = (
        widened * lax.rsqrt(jnp.mean(widened * widened, axis=-1, keepdims=True) + 1e-06)
    ).astype(jnp.bfloat16)
    preact = jnp.dot(normed, up_block, preferred_element_type=jnp.float32)
    hidden = jnp.square(jax.nn.relu(preact)).astype(jnp.bfloat16)
    summed = lax.psum_scatter(
        lax.dot_general(
            down_columns, hidden, (((0,), (1,)), ((), ())), preferred_element_type=jnp.float32
        ).astype(jnp.bfloat16),
        "fs",
        scatter_dimension=0,
        tiled=True,
    )
    mixed = summed.T
    return (up_block, down_columns, mixed)


def solution(mesh):
    in_specs = (P(("gr", "tp"), None), P("fs"), P("fs", ("gr", "tp")), P("fs", ("gr", "tp")))
    out_specs = (P(None, "fs"), P("fs", None), P(("gr", "tp"), "fs"))
    return jax.shard_map(
        per_device, mesh=mesh, in_specs=in_specs, out_specs=out_specs, check_vma=False
    )
```

profile of v0, /device:TPU:0, one launch (start us, length us, event | category | flops | bytes accessed | tf_op | source)
XLA Modules:
  0.0 242.2 jit_solution(8741351901346556773)
XLA Ops:
  7.2 0.0 all-gather.3.cloned.1.call-start
  7.2 2.7 %multiply_convert_fusion.1 = bf16[256,2048]{1,0:T(8,128)(2,1)} fusion(f32[256,2048]{1,0:T(8,128)} %param.6, f32[256]{0:T(256)} %param.5), kind=kLoop, calls=%fused_computation.10 | loop fusion | flops 1048576 | bytes 3146752 | tf_op jit(solution)/shard_map/convert_element_type | solution.py:8
  10.0 0.0 all-gather.3.cloned.1.call-update
  10.0 37.3 %all-gather.3.cloned.1.call-done = bf16[256,8192]{1,0:T(8,128)(2,1)} async-done(((bf16[256,2048]{1,0:T(8,128)(2,1)}), bf16[256,8192]{1,0:T(8,128)(2,1)}) %all-gather.3.cloned.1.call-update) | async-done | bytes 4194320 | tf_op jit(solution)/shard_map/all_gather | solution.py:11
  47.3 4.8 %copy.10 = bf16[32,8,8,1024]{3,2,0,1:T(8,128)(2,1)} copy(bf16[32,8,8,1024]{3,2,1,0:T(8,128)(2,1)} %bitcast.13) | data formatting | bytes 8388608 | tf_op jit(solution)/shard_map/all_to_all | solution.py:14
  52.1 0.0 copy-start.1
  52.1 5.6 %all-to-all-start = ((bf16[256,8,1024]{2,0,1:T(8,128)(2,1)}), bf16[256,8,1024]{2,0,1:T(8,128)(2,1)}, u32[]{:S(2)}, u32[]{:S(2)}) async-start(bf16[256,8,1024]{2,0,1:T(8,128)(2,1)} %bitcast.12), calls=%async_computation | async-start | bytes 8388608 | tf_op jit(solution)/shard_map/all_to_all | solution.py:14
  57.8 0.0 all-gather.5.cloned.1.call-start
  57.8 0.0 copy-done.1
  57.9 1.1 convert_element_type.22
  59.0 0.0 all-gather.5.cloned.1.call-update
  59.0 0.0 reduce-scatter.2.cloned.1.call-start
  59.0 2.1 fusion
  61.1 34.6 %all-gather.5.cloned.1.call-done = bf16[1024,2048]{1,0:T(8,128)(2,1)} async-done(((bf16[1024,512]{1,0:T(8,128)(2,1)}), bf16[1024,2048]{1,0:T(8,128)(2,1)}) %all-gather.5.cloned.1.call-update) | async-done | bytes 4194320 | tf_op jit(solution)/shard_map/all_gather | solution.py:12
  95.7 55.8 %all-to-all-done = bf16[256,8,1024]{2,0,1:T(8,128)(2,1)} async-done(((bf16[256,8,1024]{2,0,1:T(8,128)(2,1)}), bf16[256,8,1024]{2,0,1:T(8,128)(2,1)}, u32[]{:S(2)}, u32[]{:S(2)}) %all-to-all-start) | async-done | bytes 4194336 | tf_op jit(solution)/shard_map/all_to_all | solution.py:14
  151.5 9.9 %fusion.2 = bf16[2048,512]{0,1:T(8,128)(2,1)} fusion(bf16[1024,2048]{1,0:T(8,128)(2,1)} %all-gather.5.cloned.1.call-done, bf16[2048,1024]{1,0:T(8,128)(2,1)} %bitcast.1, bf16[512,2048]{1,0:T(8,128)(2,1)} %param.4, f32[512]{0:T(512)S(1)} %add_rsqrt_fusion), kind=kOutput, calls=%fused_computation.6 | convolution fusion | flops 4300734464 | bytes 12584960 | tf_op jit(solution)/shard_map/dot_general | solution.py:22
  161.4 0.0 reduce-scatter.2.cloned.1.call-update
  161.4 67.4 %reduce-scatter.2.cloned.1.call-done = bf16[256,512]{0,1:T(8,128)(2,1)} async-done(((bf16[2048,512]{0,1:T(8,128)(2,1)}), bf16[256,512]{0,1:T(8,128)(2,1)}) %reduce-scatter.2.cloned.1.call-update) | async-done | bytes 262160 | tf_op jit(solution)/shard_map/reduce_scatter | solution.py:21
  228.8 0.0 copy-start
  228.8 4.8 %copy.13 = bf16[2048,1024]{1,0:T(8,128)(2,1)} copy(bf16[2048,1024]{1,0:T(8,128)(2,1)} %bitcast.1) | data formatting | bytes 8388608
  233.7 0.0 copy-done
  233.7 2.0 copy.14
  (1 shorter events, 0.0 us)
Async XLA Ops:
  7.2 40.2 %all-gather.3.cloned.1.call-start = ((), (), s32[]{:S(2)}) async-start(), calls=%async_computation.2 | async-start | bytes 5242880 | tf_op jit(solution)/shard_map/all_gather | solution.py:11
  52.1 5.7 %copy-start.1 = (f32[1024,512]{1,0:T(8,128)S(1)}, f32[1024,512]{1,0:T(8,128)}, u32[]{:S(2)}) copy-start(f32[1024,512]{1,0:T(8,128)} %param.7) | copy-start | bytes 6291460
  52.1 99.3 %all-to-all-start = ((bf16[256,8,1024]{2,0,1:T(8,128)(2,1)}), bf16[256,8,1024]{2,0,1:T(8,128)(2,1)}, u32[]{:S(2)}, u32[]{:S(2)}) async-start(bf16[256,8,1024]{2,0,1:T(8,128)(2,1)} %bitcast.12), calls=%async_computation | async-start | bytes 8388608 | tf_op jit(solution)/shard_map/all_to_all | solution.py:14
  57.8 37.9 %all-gather.5.cloned.1.call-start = ((), (), s32[]{:S(2)}) async-start(), calls=%async_computation.3 | async-start | bytes 5242880 | tf_op jit(solution)/shard_map/all_gather | solution.py:12
  59.0 169.9 %reduce-scatter.2.cloned.1.call-start = ((), (), s32[]{:S(2)}) async-start(), calls=%async_computation.4 | async-start | bytes 2359296 | tf_op jit(solution)/shard_map/reduce_scatter | solution.py:21
  228.8 4.8 %copy-start = (bf16[1024,2048]{1,0:T(8,128)(2,1)S(1)}, bf16[1024,2048]{1,0:T(8,128)(2,1)}, u32[]{:S(2)}) copy-start(bf16[1024,2048]{1,0:T(8,128)(2,1)} %all-gather.5.cloned.1.call-done) | copy-start | bytes 12582916
Sparse Core Ops, SparseCore 0:
  10.1 37.1 all-gather.2
  60.7 34.9 all-gather.4
  161.6 67.2 reduce-scatter.1
where the time goes:
time: 243 us; the launch traced here: 242 us
  waiting for transfers between devices  195 us (80%)
  between operations  13.8 us (6%)
  local copies, waits for them, and re-layouts  11.7 us (5%)
  matrix products  9.92 us (4%)
  other arithmetic  5.93 us (2%)
  starting transfers between devices  5.77 us (2%)
    reduce_scatter x1, waiting for transfers between devices, per_device(): lax.psum_scatter(lax.dot_general(down_columns, hidden, (((0,), (1,)), (()...  67.4 us
    all_to_all x1, waiting for transfers between devices, per_device(): lax.all_to_all(up_columns, 'fs', split_axis=1, concat_axis=0, tiled=True)  55.8 us
    all_gather x1, waiting for transfers between devices, per_device(): lax.all_gather(up_scaled, ('gr', 'tp'), axis=1, tiled=True)  37.3 us
    all_gather x1, waiting for transfers between devices, per_device(): lax.all_gather(down_half, ('gr', 'tp'), axis=1, tiled=True)  34.6 us
    dot_general x1, matrix products, per_device(): lax.dot_general(down_columns, hidden, (((0,), (1,)), ((), ())), preferred...  9.92 us
    unnamed x6, local copies, waits for them, and re-layouts  6.83 us
    all_to_all x1, starting transfers between devices, per_device(): lax.all_to_all(up_columns, 'fs', split_axis=1, concat_axis=0, tiled=True)  5.65 us
  transfers between devices with their start and end apart: 4, of which 4 were waited for; matrix products, arithmetic and copies ran while one was open for 1% of the time, Pallas kernels for 0%

commit v1 on v0

--- a/solution.py
+++ b/solution.py
@@ -9,7 +9,7 @@
     down_half = down_weight.astype(jnp.bfloat16)
     up_columns, down_columns = (
         lax.all_gather(up_scaled, ("gr", "tp"), axis=1, tiled=True),
-        lax.all_gather(down_half, ("gr", "tp"), axis=1, tiled=True),
+        jnp.concatenate(lax.all_gather(down_half, ("gr", "tp")), axis=1),
     )
     up_block = lax.all_to_all(up_columns, "fs", split_axis=1, concat_axis=0, tiled=True)
     widened = tokens.astype(jnp.float32)

time: 243 us -> 240 us (0.988)
  waiting for transfers between devices: 195 us -> 186 us
  local copies, waits for them, and re-layouts: 11.7 us -> 18.3 us
    all_to_all x1, waiting for transfers between devices: 55.8 us -> 46.9 us  [per_device(): lax.all_to_all(up_columns, 'fs', split_axis=1, concat_axis=0, tiled=True)]
    all_gather x0 -> x1, local copies, waits for them, and re-layouts: none -> 5.42 us  [per_device(): lax.all_gather(down_half, ('gr', 'tp'))]
  transfers between devices with their start and end apart: 4 -> 4, of which waited for: 4 -> 4; matrix products, arithmetic and copies ran while one was open for 1% -> 5% of each run, Pallas kernels for 0% -> 0%
where the time goes in v1:
time: 240 us; the launch traced here: 239 us
  waiting for transfers between devices  186 us (78%)
  local copies, waits for them, and re-layouts  18.3 us (8%)
  between operations  13.8 us (6%)
  matrix products  9.33 us (4%)
  other arithmetic  5.93 us (2%)
  starting transfers between devices  5.77 us (2%)
    reduce_scatter x1, waiting for transfers between devices, per_device(): lax.psum_scatter(lax.dot_general(down_columns, hidden, (((0,), (1,)), (()...  67.1 us
    all_to_all x1, waiting for transfers between devices, per_device(): lax.all_to_all(up_columns, 'fs', split_axis=1, concat_axis=0, tiled=True)  46.9 us
    all_gather x1, waiting for transfers between devices, per_device(): lax.all_gather(up_scaled, ('gr', 'tp'), axis=1, tiled=True)  37.3 us
    all_gather x1, waiting for transfers between devices, per_device(): lax.all_gather(down_half, ('gr', 'tp'))  34.6 us
    dot_general x1, matrix products, per_device(): lax.dot_general(down_columns, hidden, (((0,), (1,)), ((), ())), preferred...  9.33 us
    unnamed x6, local copies, waits for them, and re-layouts  8.06 us
    all_to_all x1, starting transfers between devices, per_device(): lax.all_to_all(up_columns, 'fs', split_axis=1, concat_axis=0, tiled=True)  5.65 us
    all_gather x1, local copies, waits for them, and re-layouts, per_device(): lax.all_gather(down_half, ('gr', 'tp'))  5.42 us
  transfers between devices with their start and end apart: 4, of which 4 were waited for; matrix products, arithmetic and copies ran while one was open for 5% of the time, Pallas kernels for 0%

profile of v1, /device:TPU:0, one launch (start us, length us, event | category | flops | bytes accessed | tf_op | source)
XLA Modules:
  0.0 239.1 jit_solution(3171602579456428717)
XLA Ops:
  7.2 0.0 all-gather.4.cloned.1.call-start
  7.2 2.7 %multiply_convert_fusion.1 = bf16[256,2048]{1,0:T(8,128)(2,1)} fusion(f32[256,2048]{1,0:T(8,128)} %param.6, f32[256]{0:T(256)} %param.5), kind=kLoop, calls=%fused_computation.10 | loop fusion | flops 1048576 | bytes 3146752 | tf_op jit(solution)/shard_map/convert_element_type | solution.py:8
  10.0 0.0 all-gather.4.cloned.1.call-update
  10.0 37.3 %all-gather.4.cloned.1.call-done = bf16[256,8192]{1,0:T(8,128)(2,1)} async-done(((bf16[256,2048]{1,0:T(8,128)(2,1)}), bf16[256,8192]{1,0:T(8,128)(2,1)}) %all-gather.4.cloned.1.call-update) | async-done | bytes 4194320 | tf_op jit(solution)/shard_map/all_gather | solution.py:11
  47.3 4.8 %copy.12 = bf16[32,8,8,1024]{3,2,0,1:T(8,128)(2,1)} copy(bf16[32,8,8,1024]{3,2,1,0:T(8,128)(2,1)} %bitcast.21) | data formatting | bytes 8388608 | tf_op jit(solution)/shard_map/all_to_all | solution.py:14
  52.1 0.0 copy-start
  52.1 5.6 %all-to-all-start = ((bf16[256,8,1024]{2,0,1:T(8,128)(2,1)}), bf16[256,8,1024]{2,0,1:T(8,128)(2,1)}, u32[]{:S(2)}, u32[]{:S(2)}) async-start(bf16[256,8,1024]{2,0,1:T(8,128)(2,1)} %bitcast.16), calls=%async_computation | async-start | bytes 8388608 | tf_op jit(solution)/shard_map/all_to_all | solution.py:14
  57.8 0.0 all-gather.6.cloned.1.call-start
  57.8 0.0 copy-done
  57.9 1.1 convert_element_type.22
  59.0 0.0 all-gather.6.cloned.1.call-update
  59.0 0.0 reduce-scatter.2.cloned.1.call-start
  59.0 2.1 fusion
  61.1 34.6 %all-gather.6.cloned.1.call-done = bf16[4096,512]{1,0:T(8,128)(2,1)} async-done(((bf16[1024,512]{1,0:T(8,128)(2,1)}), bf16[4096,512]{1,0:T(8,128)(2,1)}) %all-gather.6.cloned.1.call-update) | async-done | bytes 4194320 | tf_op jit(solution)/shard_map/all_gather | solution.py:12
  95.7 5.4 %copy.8 = bf16[4,1024,512]{2,0,1:T(4,128)(2,1)S(1)} copy(bf16[4,1024,512]{2,1,0:T(8,128)(2,1)} %bitcast.20) | data formatting | bytes 8388608 | tf_op jit(solution)/shard_map/all_gather | solution.py:12
  101.1 0.0 copy-start.1
  101.1 3.4 %copy.10 = bf16[128,8,4,512]{3,1,2,0:T(8,128)(2,1)} copy(bf16[128,8,4,512]{3,2,1,0:T(4,128)(2,1)S(1)} %bitcast.17) | data formatting | bytes 8388608
  104.6 46.9 %all-to-all-done = bf16[256,8,1024]{2,0,1:T(8,128)(2,1)} async-done(((bf16[256,8,1024]{2,0,1:T(8,128)(2,1)}), bf16[256,8,1024]{2,0,1:T(8,128)(2,1)}, u32[]{:S(2)}, u32[]{:S(2)}) %all-to-all-start) | async-done | bytes 4194336 | tf_op jit(solution)/shard_map/all_to_all | solution.py:14
  151.5 0.0 copy-done.1
  151.5 9.3 %fusion.2 = bf16[2048,512]{0,1:T(8,128)(2,1)} fusion(bf16[1024,2048]{1,0:T(8,128)(2,1)} %bitcast.18, bf16[2048,1024]{1,0:T(8,128)(2,1)} %bitcast.1, bf16[512,2048]{1,0:T(8,128)(2,1)S(1)} %copy-done.1, f32[512]{0:T(512)S(1)} %add_rsqrt_fusion), kind=kOutput, calls=%fused_computation.6 | convolution fusion | flops 4300734464 | bytes 12584960 | tf_op jit(solution)/shard_map/dot_general | solution.py:22
  160.8 0.0 reduce-scatter.2.cloned.1.call-update
  160.8 67.1 %reduce-scatter.2.cloned.1.call-done = bf16[256,512]{0,1:T(8,128)(2,1)} async-done(((bf16[2048,512]{0,1:T(8,128)(2,1)}), bf16[256,512]{0,1:T(8,128)(2,1)}) %reduce-scatter.2.cloned.1.call-update) | async-done | bytes 262160 | tf_op jit(solution)/shard_map/reduce_scatter | solution.py:21
  228.0 4.6 %copy.14 = bf16[2048,1024]{1,0:T(8,128)(2,1)} copy(bf16[2048,1024]{1,0:T(8,128)(2,1)} %bitcast.1) | data formatting | bytes 8388608
  (1 shorter events, 0.0 us)
Async XLA Ops:
  7.2 40.2 %all-gather.4.cloned.1.call-start = ((), (), s32[]{:S(2)}) async-start(), calls=%async_computation.2 | async-start | bytes 5242880 | tf_op jit(solution)/shard_map/all_gather | solution.py:11
  52.1 5.7 %copy-start = (f32[1024,512]{1,0:T(8,128)S(1)}, f32[1024,512]{1,0:T(8,128)}, u32[]{:S(2)}) copy-start(f32[1024,512]{1,0:T(8,128)} %param.7) | copy-start | bytes 6291460
  52.1 99.3 %all-to-all-start = ((bf16[256,8,1024]{2,0,1:T(8,128)(2,1)}), bf16[256,8,1024]{2,0,1:T(8,128)(2,1)}, u32[]{:S(2)}, u32[]{:S(2)}) async-start(bf16[256,8,1024]{2,0,1:T(8,128)(2,1)} %bitcast.16), calls=%async_computation | async-start | bytes 8388608 | tf_op jit(solution)/shard_map/all_to_all | solution.py:14
  57.8 37.9 %all-gather.6.cloned.1.call-start = ((), (), s32[]{:S(2)}) async-start(), calls=%async_computation.4 | async-start | bytes 5242880 | tf_op jit(solution)/shard_map/all_gather | solution.py:12
  59.0 169.0 %reduce-scatter.2.cloned.1.call-start = ((), (), s32[]{:S(2)}) async-start(), calls=%async_computation.3 | async-start | bytes 2359296 | tf_op jit(solution)/shard_map/reduce_scatter | solution.py:21
  101.1 50.4 %copy-start.1 = (bf16[512,2048]{1,0:T(8,128)(2,1)S(1)}, bf16[512,2048]{1,0:T(8,128)(2,1)}, u32[]{:S(2)}) copy-start(bf16[512,2048]{1,0:T(8,128)(2,1)} %param.4) | copy-start | bytes 6291460
Sparse Core Ops, SparseCore 0:
  10.1 37.1 all-gather.3
  60.7 34.9 all-gather.5
  161.0 66.9 reduce-scatter.1
